TPU v7x, 512 devices: a whole 4x4x16 slice. The times are simulated.
512 devices in a mesh: sp: 16 (over z), fs: 4 (over y), tp: 8 (over x, core).
Axes of the slice: x: 4, y: 4, z: 16, core: 2. Of those that a mesh axis runs over, the one named last changes fastest.
Arguments:
- tokens: bfloat16 [4, 16384, 2048], P('fs', 'sp', 'tp'), may hold values from -8 to 8
- norm_gain: float32 [2048], replicated, may hold values from 0.1 to 1.9
- w_query: bfloat16 [2048, 1024], P(('sp', 'fs'), 'tp'), may hold values from -4 to 4
- w_key: bfloat16 [2048, 512], P(('sp', 'fs'), 'tp'), may hold values from -0.16 to 0.16
- w_value: bfloat16 [2048, 512], P(('sp', 'fs'), 'tp'), may hold values from -0.125 to 0.125
- w_conv_in: bfloat16 [2048, 1024], P(('sp', 'fs'), 'tp'), may hold values from -0.125 to 0.125
- w_conv_b: bfloat16 [2048, 1024], P(('sp', 'fs'), 'tp'), may hold values from -0.125 to 0.125
- w_conv_c: bfloat16 [2048, 1024], P(('sp', 'fs'), 'tp'), may hold values from -0.125 to 0.125
- conv_taps: bfloat16 [3, 1024], P(None, 'tp'), may hold values from -3.5 to 3.5
- sink_logits: float32 [16], P('tp'), may hold values from 1 to 5
- w_attn_out: bfloat16 [1024, 2048], P('tp', ('sp', 'fs')), may hold values from -0.375 to 0.375
- w_conv_out: bfloat16 [1024, 2048], P('tp', ('sp', 'fs')), may hold values from -0.125 to 0.125
Outputs:
- mixed: bfloat16 [4, 16384, 2048], P('fs', ('sp', 'tp'))
All inputs are finite; a program needn't handle non-finite values.
Results may differ from a plain program's by a relative error of at most 0.02.
Values may be sent and summed in bfloat16 or wider, within the bound.
A program may use at most 128 MiB of HBM per device.

v0:
```python
import jax
import jax.numpy as jnp
from jax import lax
from jax.sharding import PartitionSpec as P

HEADS = 16
HEAD = 64
WINDOW = 128


def in_one_piece(arrays, axis, dim, along):
    widths = [a.shape[along] for a in arrays]
    both = jnp.concatenate(arrays, axis=along)
    whole = lax.all_gather(both, axis, axis=dim, tiled=True)
    return tuple(jnp.split(whole, [sum(widths[:k]) for k in range(1, len(widths))], axis=along))


def shifted(block, axis, distance):
    devices = range(lax.axis_size(axis))
    route = [(i - distance, i) for i in devices if i - distance in devices]
    return lax.ppermute(block, axis, route)


def rows_first(arrays, axis, dims):
    turned = [jnp.moveaxis(a, dim, 0) for a, dim in zip(arrays, dims)]
    both = jnp.concatenate([t.reshape(len(t), -1) for t in turned], axis=1)
    whole, at, finished = (lax.all_gather(both, axis, axis=0, tiled=True), 0, [])
    for t, dim in zip(turned, dims):
        share = whole[:, at : at + t[0].size].reshape(-1, *t.shape[1:])
        finished.append(jnp.moveaxis(share, 0, dim))
        at += t[0].size
    return tuple(finished)


def norm_rows(tokens, norm_gain):
    values = tokens.astype(jnp.float32)
    average = jnp.mean(values, axis=-1, keepdims=True)
    centred = values - average
    variance = jnp.mean(centred * centred, axis=-1, keepdims=True)
    return (centred * lax.rsqrt(variance + 1e-05) * norm_gain).astype(jnp.bfloat16)


def attend(queries, keys_values, earlier_rows, sink_logits, head_base, row_base):
    row_total = queries.shape[0]
    kv_cols = keys_values.shape[1] // 2
    kv_here = kv_cols // HEAD
    heads_here = queries.shape[1] // HEAD
    group = heads_here // kv_here
    keys_all = jnp.concatenate([earlier_rows, keys_values], axis=0)
    block_rows = min(512, row_total)
    head_ids = head_base + jnp.arange(heads_here, dtype=jnp.int32)
    slopes = jnp.exp2(-8.0 * (head_ids + 1).astype(jnp.float32) / HEADS).reshape(kv_here, group)[
        :, :, None, None
    ]
    sinks = sink_logits.reshape(kv_here, group)[:, :, None, None]
    row_ids = jnp.arange(block_rows, dtype=jnp.int32)[:, None]
    col_ids = jnp.arange(block_rows + WINDOW, dtype=jnp.int32)[None, :]
    distance = WINDOW + row_ids - col_ids
    outputs = []
    for block in range(row_total // block_rows):
        first_row = block * block_rows
        query_block = queries[first_row : first_row + block_rows].reshape(
            block_rows, kv_here, group, HEAD
        )
        band = keys_all[first_row : first_row + block_rows + WINDOW]
        band_keys = band[:, :kv_cols].reshape(block_rows + WINDOW, kv_here, HEAD)
        band_values = band[:, kv_cols:].reshape(block_rows + WINDOW, kv_here, HEAD)
        scores = jnp.einsum(
            "qkgd,skd->kgqs", query_block, band_keys, preferred_element_type=jnp.float32
        ) * HEAD ** (-0.5)
        scores = scores - slopes * distance.astype(jnp.float32)
        key_place = row_base + first_row - WINDOW + col_ids
        keep = (distance >= 0) & (distance < WINDOW) & (key_place >= 0)
        scores = jnp.where(keep, scores, -jnp.inf)
        highest = jnp.maximum(jnp.max(scores, axis=-1, keepdims=True), sinks)
        raised = jnp.exp(scores - highest)
        denominator = jnp.sum(raised, axis=-1, keepdims=True) + jnp.exp(sinks - highest)
        weights = (raised / denominator).astype(jnp.bfloat16)
        mixed = jnp.einsum(
            "kgqs,skd->qkgd", weights, band_values, preferred_element_type=jnp.float32
        )
        outputs.append(mixed.astype(jnp.bfloat16).reshape(block_rows, heads_here * HEAD))
    return jnp.concatenate(outputs, axis=0)


def on_device(
    tokens,
    norm_gain,
    w_query,
    w_key,
    w_value,
    w_conv_in,
    w_conv_b,
    w_conv_c,
    conv_taps,
    sink_logits,
    w_attn_out,
    w_conv_out,
):
    gathered = lax.all_gather(tokens, "tp", axis=2, tiled=True)[0]
    normed = norm_rows(gathered, norm_gain)
    row_total = normed.shape[0]
    weight_rows = in_one_piece(
        (w_query, w_key, w_value, w_conv_in, w_conv_b, w_conv_c), ("sp", "fs"), 0, 1
    )
    results = tuple(
        (
            jnp.dot(normed, rows_part, preferred_element_type=jnp.float32)
            for rows_part in weight_rows
        )
    )
    queries, keys, values, inner, gate_b, gate_c = tuple(
        (result.astype(jnp.bfloat16) for result in results)
    )
    product = (gate_c.astype(jnp.float32) * inner.astype(jnp.float32)).astype(jnp.bfloat16)
    keys_values = jnp.concatenate([keys, values], axis=1)
    earlier_kv, earlier_product = shifted(
        (keys_values[row_total - WINDOW :], product[row_total - 2 :]), "sp", 1
    )
    heads_here = queries.shape[1] // HEAD
    head_base = lax.axis_index("tp") * heads_here
    row_base = lax.axis_index("sp") * row_total
    attended = attend(queries, keys_values, earlier_kv, sink_logits, head_base, row_base)
    taps = conv_taps.astype(jnp.float32)
    padded = jnp.concatenate([earlier_product, product], axis=0).astype(jnp.float32)
    filtered = (
        taps[0] * padded[0:row_total]
        + taps[1] * padded[1 : row_total + 1]
        + taps[2] * padded[2 : row_total + 2]
    )
    conv_out = (gate_b.astype(jnp.float32) * filtered).astype(jnp.bfloat16)
    attn_columns, conv_columns = rows_first((w_attn_out, w_conv_out), ("sp", "fs"), (1, 1))
    summed = lax.psum_scatter(
        (
            jnp.dot(attended, attn_columns, preferred_element_type=jnp.float32)
            + jnp.dot(conv_out, conv_columns, preferred_element_type=jnp.float32)
        ).astype(jnp.bfloat16),
        "tp",
        scatter_dimension=0,
        tiled=True,
    )
    return summed[None]


def solution(mesh):
    placed = (
        P("fs", "sp", "tp"),
        P(),
        P(("sp", "fs"), "tp"),
        P(("sp", "fs"), "tp"),
        P(("sp", "fs"), "tp"),
        P(("sp", "fs"), "tp"),
        P(("sp", "fs"), "tp"),
        P(("sp", "fs"), "tp"),
        P(None, "tp"),
        P("tp"),
        P("tp", ("sp", "fs")),
        P("tp", ("sp", "fs")),
    )
    return jax.shard_map(
        on_device,
        mesh=mesh,
        in_specs=placed,
        out_specs=P("fs", ("sp", "tp"), None),
        check_vma=False,
    )
```

profile of v0, /device:TPU:8, one launch (start us, length us, event | category | flops | bytes accessed | tf_op | source)
XLA Modules:
  0.0 406.5 jit_solution(2349871307167087293)
XLA Ops:
  6.5 0.7 all-gather.4.cloned.1.call-update
  7.3 1.5 concatenate.18
  8.9 1.3 pad_maximum_fusion.4
  10.3 0.7 convert_element_type.108
  11.0 1.2 fusion.14
  12.2 0.5 fusion.32
  12.7 44.3 %all-gather.4.cloned.1.call-done = bf16[1,1024,2048]{2,1,0:T(8,128)(2,1)} async-done(((bf16[1,1024,256]{2,1,0:T(8,128)(2,1)}), bf16[1,1024,2048]{2,1,0:T(8,128)(2,1)}) %all-gather.4.cloned.1.call-update) | async-done | bytes 4194320 | tf_op jit(solution)/shard_map/all_gather | solution.py:100
  57.0 3.0 convert_reduce_fusion
  60.0 0.5 copy-done.1
  60.5 1.2 fusion.3
  61.7 3.0 fusion.5
  64.7 137.2 %all-gather.6.cloned.1.call-done = bf16[2048,640]{1,0:T(8,128)(2,1)} async-done(((bf16[32,640]{1,0:T(8,128)(2,1)}), bf16[2048,640]{1,0:T(8,128)(2,1)}) %all-gather.6.cloned.1.call-update) | async-done | bytes 2621456 | tf_op jit(solution)/shard_map/all_gather | solution.py:14
  201.9 3.9 convolution_convert_fusion.4
  205.8 2.6 convolution_convert_fusion.5
  208.4 3.7 collective-permute-start
  212.1 1.5 convolution_convert_fusion.3
  213.7 1.2 fusion.21
  214.9 1.3 fusion.20
  216.2 2.4 collective-permute-start.1
  218.7 0.9 fusion.65
  219.5 0.2 collective-permute-done.1
  219.8 0.9 fusion.64
  220.8 0.4 fusion.8
  221.1 0.1 exponential_add_fusion.1
  221.2 0.4 fusion.9
  221.6 0.1 exponential_add_fusion
  221.7 0.6 fusion.28
  222.3 0.6 fusion.25
  222.8 117.6 %all-gather.8.cloned.1.call-done = bf16[2048,256]{1,0:T(8,128)(2,1)} async-done(((bf16[32,256]{1,0:T(8,128)(2,1)}), bf16[2048,256]{1,0:T(8,128)(2,1)}) %all-gather.8.cloned.1.call-update) | async-done | bytes 1048592 | tf_op jit(solution)/shard_map/all_gather | solution.py:27
  340.4 5.6 %fusion.42 = f32[1024,2048]{1,0:T(8,128)} fusion(bf16[2048,256]{1,0:T(8,128)(2,1)} %all-gather.8.cloned.1.call-done, bf16[512,128]{0,1:T(8,128)(2,1)S(1)} %bitcast.77, bf16[512,128]{0,1:T(8,128)(2,1)S(1)} %bitcast.78), kind=kOutput, calls=%fused_computation.54 | convolution fusion | flops 537395200 | bytes 9175040 | tf_op jit(solution)/shard_map/dot_general | solution.py:135
  345.9 11.1 %add_convert_fusion = bf16[1024,2048]{1,0:T(8,128)(2,1)} fusion(f32[1024,2048]{1,0:T(8,128)} %fusion.42, bf16[1024,2048]{1,0:T(8,128)(2,1)} %fusion.5, bf16[2048,256]{1,0:T(8,128)(2,1)} %all-gather.8.cloned.1.call-done, f32[1026,128]{1,0:T(8,128)S(1)} %maximum_convert_fusion, bf16[2048,640]{1,0:T(8,128)(2,1)S(1)} %copy-done.2, f32[128]{0:T(128)S(1)} %get-tuple-element.8, ...), kind=kOutput, calls=%fused_computation.8 | convolution fusion | flops 1079115776 | bytes 19400192 | tf_op jit(solution)/shard_map/dot_general | solution.py:136
  357.1 42.9 %reduce-scatter.2.cloned.1.call-done = bf16[128,2048]{1,0:T(8,128)(2,1)} async-done(((bf16[1024,2048]{1,0:T(8,128)(2,1)}), bf16[128,2048]{1,0:T(8,128)(2,1)}) %reduce-scatter.2.cloned.1.call-update) | async-done | bytes 524304 | tf_op jit(solution)/shard_map/reduce_scatter | solution.py:133
  (30 shorter events, 0.4 us)
Async XLA Ops:
  6.5 50.5 %all-gather.4.cloned.1.call-start = ((), (), s32[]{:S(2)}) async-start(), calls=%async_computation.1 | async-start | bytes 4718592 | tf_op jit(solution)/shard_map/all_gather | solution.py:100
  7.3 194.6 %all-gather.6.cloned.1.call-start = ((), (), s32[]{:S(2)}) async-start(), calls=%async_computation.2 | async-start | bytes 2662400 | tf_op jit(solution)/shard_map/all_gather | solution.py:14
  8.8 331.6 %all-gather.8.cloned.1.call-start = ((), (), s32[]{:S(2)}) async-start(), calls=%async_computation.3 | async-start | bytes 1064960 | tf_op jit(solution)/shard_map/all_gather | solution.py:27
  10.2 389.8 %reduce-scatter.2.cloned.1.call-start = ((), (), s32[]{:S(2)}) async-start(), calls=%async_computation.4 | async-start | bytes 4718592 | tf_op jit(solution)/shard_map/reduce_scatter | solution.py:133
  57.0 3.4 copy-start.1
  60.0 1.7 copy-start.4
  201.9 3.9 copy-start
  205.8 6.3 %copy-start.2 = (bf16[2048,640]{1,0:T(8,128)(2,1)S(1)}, bf16[2048,640]{1,0:T(8,128)(2,1)}, u32[]{:S(2)}) copy-start(bf16[2048,640]{1,0:T(8,128)(2,1)} %all-gather.6.cloned.1.call-done) | copy-start | bytes 7864324
  208.4 11.4 %collective-permute-start = (bf16[128,128]{0,1:T(8,128)(2,1)S(1)}, bf16[128,128]{0,1:T(8,128)(2,1)S(1)}, u32[]{:S(2)}, u32[]{:S(2)}) collective-permute-start(bf16[128,128]{0,1:T(8,128)(2,1)S(1)} %pad_maximum_fusion.3), channel_id=1, source_target_pairs={{0,32},{32,64},{64,96},{96,128},{128,160},{160,192},{192,224},{224... | collective-permute-start | bytes 98312 | tf_op jit(solution)/shard_map/ppermute | solution.py:21
  214.9 3.7 copy-start.3
  216.2 3.5 collective-permute-start.1
  219.5 1.2 copy-start.5
Sparse Core Ops, SparseCore 0:
  9.4 47.5 all-gather.3
  60.0 141.8 all-gather.5
  204.8 135.5 all-gather.7
  357.2 42.6 reduce-scatter.1
where the time goes:
time: 407 us; the launch traced here: 406 us
  waiting for transfers between devices  343 us (84%)
  matrix products  30.1 us (7%)
  between operations  13.3 us (3%)
  other arithmetic  12 us (3%)
  starting transfers between devices  6.25 us (2%)
    all_gather x1, waiting for transfers between devices, in_one_piece(): whole = lax.all_gather(both, axis, axis=dim, tiled=True)  137 us
    all_gather x1, waiting for transfers between devices, rows_first(): lax.all_gather(both, axis, axis=0, tiled=True)  118 us
    all_gather x1, waiting for transfers between devices, on_device(): gathered = lax.all_gather(tokens, 'tp', axis=2, tiled=True)[0]  44.3 us
    reduce_scatter x1, waiting for transfers between devices, on_device(): lax.psum_scatter((jnp.dot(attended, attn_columns, preferred_element_type=...  42.9 us
    dot_general x1, matrix products, on_device(): jnp.dot(conv_out, conv_columns, preferred_element_type=jnp.float32)  11.1 us
    dot_general x5, matrix products, on_device(): jnp.dot(normed, rows_part, preferred_element_type=jnp.float32)  10.5 us
  transfers between devices with their start and end apart: 6, of which 5 were waited for; matrix products, arithmetic and copies ran while one was open for 7% of the time, Pallas kernels for 0%

commit v1 on v0

--- a/solution.py
+++ b/solution.py
@@ -6,6 +6,14 @@
 HEADS = 16
 HEAD = 64
 WINDOW = 128
+
+
+def gather_by_exchange(array, axis, dim):
+    count = lax.axis_size(axis)
+    repeats = [count if d == dim else 1 for d in range(array.ndim)]
+    return lax.all_to_all(
+        jnp.tile(array, repeats), axis, split_axis=dim, concat_axis=dim, tiled=True
+    )
 
 
 def in_one_piece(arrays, axis, dim, along):
@@ -97,7 +105,7 @@
     w_attn_out,
     w_conv_out,
 ):
-    gathered = lax.all_gather(tokens, "tp", axis=2, tiled=True)[0]
+    gathered = gather_by_exchange(tokens, "tp", 2)[0]
     normed = norm_rows(gathered, norm_gain)
     row_total = normed.shape[0]
     weight_rows = in_one_piece(

time: 407 us -> 361 us (0.89)
  waiting for transfers between devices: 343 us -> 196 us
  other arithmetic: 12 us -> 59.8 us
  local copies, waits for them, and re-layouts: 2.01 us -> 49.2 us
  starting transfers between devices: 6.25 us -> 12.6 us
    all_gather x1, waiting for transfers between devices: 137 us -> 0.01 us  [in_one_piece(): whole = lax.all_gather(both, axis, axis=dim, tiled=True)]
    all_to_all x0 -> x1, waiting for transfers between devices: none -> 48.1 us  [gather_by_exchange(): lax.all_to_all(jnp.tile(array, repeats), axis, split_axis=dim, concat_axi...]
    all_gather x1 -> x0, waiting for transfers between devices: 44.3 us -> none  [on_device(): gathered = lax.all_gather(tokens, 'tp', axis=2, tiled=True)[0]]
    another operation x0 -> x3, local copies, waits for them, and re-layouts: none -> 30.5 us  [gather_by_exchange(): jnp.tile(array, repeats)]
    unnamed x0 -> x1, other arithmetic: none -> 25.9 us
    unnamed x12 -> x21, local copies, waits for them, and re-layouts: 0.5 us -> 17.2 us
    reduce_sum x1, other arithmetic: 2.95 us -> 17.5 us  [norm_rows(): average = jnp.mean(values, axis=-1, keepdims=True)]
    all_gather x1, waiting for transfers between devices: 118 us -> 105 us  [rows_first(): lax.all_gather(both, axis, axis=0, tiled=True)]
  transfers between devices with their start and end apart: 6 -> 6, of which waited for: 5 -> 4; matrix products, arithmetic and copies ran while one was open for 7% -> 33% of each run, Pallas kernels for 0% -> 0%
where the time goes in v1:
time: 361 us; the launch traced here: 360 us
  waiting for transfers between devices  196 us (54%)
  other arithmetic  59.8 us (17%)
  local copies, waits for them, and re-layouts  49.2 us (14%)
  matrix products  28.7 us (8%)
  between operations  13.4 us (4%)
  starting transfers between devices  12.6 us (3%)
    all_gather x1, waiting for transfers between devices, rows_first(): lax.all_gather(both, axis, axis=0, tiled=True)  105 us
    all_to_all x1, waiting for transfers between devices, gather_by_exchange(): lax.all_to_all(jnp.tile(array, repeats), axis, split_axis=dim, concat_axi...  48.1 us
    reduce_scatter x1, waiting for transfers between devices, on_device(): lax.psum_scatter((jnp.dot(attended, attn_columns, preferred_element_type=...  42.9 us
    another operation x3, local copies, waits for them, and re-layouts, gather_by_exchange(): jnp.tile(array, repeats)  30.5 us
    unnamed x1, other arithmetic  25.9 us
    reduce_sum x1, other arithmetic, norm_rows(): average = jnp.mean(values, axis=-1, keepdims=True)  17.5 us
    unnamed x21, local copies, waits for them, and re-layouts  17.2 us
    dot_general x1, matrix products, on_device(): jnp.dot(conv_out, conv_columns, preferred_element_type=jnp.float32)  11.2 us
  transfers between devices with their start and end apart: 6, of which 4 were waited for; matrix products, arithmetic and copies ran while one was open for 33% of the time, Pallas kernels for 0%

profile of v1, /device:TPU:8, one launch (start us, length us, event | category | flops | bytes accessed | tf_op | source)
XLA Modules:
  0.0 360.1 jit_solution(1863694634059414918)
XLA Ops:
  6.5 1.5 concatenate.18
  8.0 1.2 copy.18
  9.3 0.5 tile.12
  9.8 28.7 %copy.31 = bf16[1,1024,2048]{1,0,2:T(2,128)(2,1)} copy(bf16[1,1024,2048]{1,2,0:T(8,128)(2,1)S(1)} %bitcast.78) | data formatting | bytes 8388608 | tf_op jit(solution)/shard_map/tile | solution.py:15
  38.6 0.5 broadcast.214
  39.1 25.9 %reduce.5 = bf16[2048,1024]{1,0:T(8,128)(2,1)} reduce(bf16[2048,1,1024]{2,1,0:T(2,128)(2,1)} %bitcast.77, bf16[]{:T(256)} %broadcast.214), dimensions={1}, to_apply=%bitcast.76.reduce_sub_computation | reduce | bytes 8388610
  64.9 7.8 %reshape.255 = bf16[8,2,131072]{2,1,0:T(2,128)(2,1)} reshape(bf16[2048,1024]{1,0:T(8,128)(2,1)} %reduce.5) | data formatting | bytes 8388608
  72.7 4.7 %all-to-all-start = ((bf16[8,2,131072]{2,1,0:T(2,128)(2,1)}), bf16[8,2,131072]{2,1,0:T(2,128)(2,1)}, u32[]{:S(2)}, u32[]{:S(2)}) async-start(bf16[8,2,131072]{2,1,0:T(2,128)(2,1)} %reshape.255), calls=%async_computation | async-start | bytes 8388608 | tf_op jit(solution)/shard_map/all_to_all | solution.py:14
  77.5 0.6 pad_maximum_fusion.4
  78.3 0.5 fusion.26
  79.0 48.1 %all-to-all-done = bf16[8,2,131072]{2,1,0:T(2,128)(2,1)} async-done(((bf16[8,2,131072]{2,1,0:T(2,128)(2,1)}), bf16[8,2,131072]{2,1,0:T(2,128)(2,1)}, u32[]{:S(2)}, u32[]{:S(2)}) %all-to-all-start) | async-done | bytes 4194336 | tf_op jit(solution)/shard_map/all_to_all | solution.py:14
  127.1 8.8 %reshape.256 = bf16[2048,1,1024]{2,1,0:T(2,128)(2,1)} reshape(bf16[8,2,131072]{2,1,0:T(2,128)(2,1)} %all-to-all-done) | data formatting | bytes 8388608
  135.9 10.1 %bitcast_convert_fusion = f32[1,1024,2048]{1,0,2:T(1,128)S(1)} fusion(bf16[2048,1,1024]{2,1,0:T(2,128)(2,1)} %reshape.256), kind=kLoop, calls=%fused_computation.94 | loop fusion | flops 2097152 | bytes 12582912 | tf_op jit(solution)/shard_map/convert_element_type | solution.py:44
  146.0 17.5 %convert_reduce_fusion = f32[1024]{0:T(1024)S(1)} fusion(bf16[2048,1,1024]{2,1,0:T(2,128)(2,1)S(1)} %copy-done.1), kind=kLoop, calls=%fused_computation.90 | loop fusion | flops 4193280 | bytes 4198400 | tf_op jit(solution)/shard_map/reduce_sum | solution.py:45
  163.6 1.2 multiply_reduce_fusion
  164.8 2.7 multiply_convert_fusion
  167.6 3.5 convolution_convert_fusion.4
  171.2 2.1 convolution_convert_fusion.5
  173.3 4.0 %collective-permute-start = (bf16[128,128]{0,1:T(8,128)(2,1)S(1)}, bf16[128,128]{0,1:T(8,128)(2,1)S(1)}, u32[]{:S(2)}, u32[]{:S(2)}) collective-permute-start(bf16[128,128]{0,1:T(8,128)(2,1)S(1)} %pad_maximum_fusion.3), channel_id=1, source_target_pairs={{0,32},{32,64},{64,96},{96,128},{128,160},{160,192},{192,224},{224... | collective-permute-start | bytes 98312 | tf_op jit(solution)/shard_map/ppermute | solution.py:29
  177.3 0.8 convolution_convert_fusion.3
  178.1 1.3 fusion.15
  179.4 1.3 fusion.14
  180.7 3.8 %collective-permute-start.1 = (bf16[2,128]{1,0:T(2,128)(2,1)S(1)}, bf16[2,128]{1,0:T(2,128)(2,1)S(1)}, u32[]{:S(2)}, u32[]{:S(2)}) collective-permute-start(bf16[2,128]{1,0:T(2,128)(2,1)S(1)} %slice.77), channel_id=1, source_target_pairs={{0,32},{32,64},{64,96},{96,128},{128,160},{160,192},{192,224},{224... | collective-permute-start | bytes 1544 | tf_op jit(solution)/shard_map/ppermute | solution.py:29
  184.6 0.9 fusion.59
  185.5 0.4 collective-permute-done.1
  185.9 0.9 fusion.58
  187.8 0.6 fusion.22
  188.4 0.6 fusion.19
  189.0 104.9 %all-gather.5.cloned.1.call-done = bf16[2048,256]{1,0:T(8,128)(2,1)} async-done(((bf16[32,256]{1,0:T(8,128)(2,1)}), bf16[2048,256]{1,0:T(8,128)(2,1)}) %all-gather.5.cloned.1.call-update) | async-done | bytes 1048592 | tf_op jit(solution)/shard_map/all_gather | solution.py:35
  293.9 5.7 %fusion.36 = f32[1024,2048]{1,0:T(8,128)} fusion(bf16[2048,256]{1,0:T(8,128)(2,1)} %all-gather.5.cloned.1.call-done, bf16[512,128]{0,1:T(8,128)(2,1)S(1)} %bitcast.80, bf16[512,128]{0,1:T(8,128)(2,1)S(1)} %bitcast.81), kind=kOutput, calls=%fused_computation.49 | convolution fusion | flops 537395200 | bytes 9175040 | tf_op jit(solution)/shard_map/dot_general | solution.py:143
  299.6 11.2 %add_convert_fusion = bf16[1024,2048]{1,0:T(8,128)(2,1)} fusion(f32[1024,2048]{1,0:T(8,128)} %fusion.36, bf16[1024,2048]{0,1:T(8,128)(2,1)} %multiply_convert_fusion, bf16[2048,256]{1,0:T(8,128)(2,1)S(1)} %copy-done.2, f32[1026,128]{1,0:T(8,128)S(1)} %maximum_convert_fusion, bf16[2048,640]{1,0:T(8,128)(2,1)} %all-gather.3.cloned.1.call-done, ...), kind=kOutput, calls=%fused_computation.1 | convolution fusion | flops 1079115776 | bytes 19400192 | tf_op jit(solution)/shard_map/dot_general | solution.py:144
  310.7 42.9 %reduce-scatter.2.cloned.1.call-done = bf16[128,2048]{1,0:T(8,128)(2,1)} async-done(((bf16[1024,2048]{1,0:T(8,128)(2,1)}), bf16[128,2048]{1,0:T(8,128)(2,1)}) %reduce-scatter.2.cloned.1.call-update) | async-done | bytes 524304 | tf_op jit(solution)/shard_map/reduce_scatter | solution.py:141
  (43 shorter events, 1.6 us)
Async XLA Ops:
  6.5 161.0 %all-gather.3.cloned.1.call-start = ((), (), s32[]{:S(2)}) async-start(), calls=%async_computation.2 | async-start | bytes 2662400 | tf_op jit(solution)/shard_map/all_gather | solution.py:22
  72.7 4.8 %copy-start.5 = (bf16[128,32]{0,1:T(8,128)(2,1)S(1)}, bf16[128,32]{0,1:T(8,128)(2,1)}, u32[]{:S(2)}) copy-start(bf16[128,32]{0,1:T(8,128)(2,1)} %param.23) | copy-start | bytes 24580
  72.7 4.8 %copy-start.6 = (bf16[128,32]{0,1:T(8,128)(2,1)S(1)}, bf16[128,32]{0,1:T(8,128)(2,1)}, u32[]{:S(2)}) copy-start(bf16[128,32]{0,1:T(8,128)(2,1)} %param.22) | copy-start | bytes 24580
  72.7 5.6 %copy-start.8 = (bf16[3,128]{1,0:T(4,128)(2,1)S(1)}, bf16[3,128]{1,0:T(4,128)(2,1)}, u32[]{:S(2)}) copy-start(bf16[3,128]{1,0:T(4,128)(2,1)} %param.20) | copy-start | bytes 2308
  72.7 54.4 %all-to-all-start = ((bf16[8,2,131072]{2,1,0:T(2,128)(2,1)}), bf16[8,2,131072]{2,1,0:T(2,128)(2,1)}, u32[]{:S(2)}, u32[]{:S(2)}) async-start(bf16[8,2,131072]{2,1,0:T(2,128)(2,1)} %reshape.255), calls=%async_computation | async-start | bytes 8388608 | tf_op jit(solution)/shard_map/all_to_all | solution.py:14
  77.4 216.4 %all-gather.5.cloned.1.call-start = ((), (), s32[]{:S(2)}) async-start(), calls=%async_computation.3 | async-start | bytes 1064960 | tf_op jit(solution)/shard_map/all_gather | solution.py:35
  78.2 275.4 %reduce-scatter.2.cloned.1.call-start = ((), (), s32[]{:S(2)}) async-start(), calls=%async_computation.4 | async-start | bytes 4718592 | tf_op jit(solution)/shard_map/reduce_scatter | solution.py:141
  135.9 10.2 %copy-start.1 = (bf16[2048,1,1024]{2,1,0:T(2,128)(2,1)S(1)}, bf16[2048,1,1024]{2,1,0:T(2,128)(2,1)}, u32[]{:S(2)}) copy-start(bf16[2048,1,1024]{2,1,0:T(2,128)(2,1)} %reshape.256) | copy-start | bytes 12582916
  163.6 1.3 copy-start.4
  167.6 3.6 %copy-start = (bf16[1024,2048]{0,1:T(8,128)(2,1)S(1)}, bf16[1024,2048]{0,1:T(8,128)(2,1)}, u32[]{:S(2)}) copy-start(bf16[1024,2048]{0,1:T(8,128)(2,1)} %multiply_convert_fusion) | copy-start | bytes 12582916
  171.2 6.1 %copy-start.3 = (bf16[2048,640]{1,0:T(8,128)(2,1)S(1)}, bf16[2048,640]{1,0:T(8,128)(2,1)}, u32[]{:S(2)}) copy-start(bf16[2048,640]{1,0:T(8,128)(2,1)} %all-gather.3.cloned.1.call-done) | copy-start | bytes 7864324
  173.3 12.6 %collective-permute-start = (bf16[128,128]{0,1:T(8,128)(2,1)S(1)}, bf16[128,128]{0,1:T(8,128)(2,1)S(1)}, u32[]{:S(2)}, u32[]{:S(2)}) collective-permute-start(bf16[128,128]{0,1:T(8,128)(2,1)S(1)} %pad_maximum_fusion.3), channel_id=1, source_target_pairs={{0,32},{32,64},{64,96},{96,128},{128,160},{160,192},{192,224},{224... | collective-permute-start | bytes 98312 | tf_op jit(solution)/shard_map/ppermute | solution.py:29
  180.7 5.1 %collective-permute-start.1 = (bf16[2,128]{1,0:T(2,128)(2,1)S(1)}, bf16[2,128]{1,0:T(2,128)(2,1)S(1)}, u32[]{:S(2)}, u32[]{:S(2)}) collective-permute-start(bf16[2,128]{1,0:T(2,128)(2,1)S(1)} %slice.77), channel_id=1, source_target_pairs={{0,32},{32,64},{64,96},{96,128},{128,160},{160,192},{192,224},{224... | collective-permute-start | bytes 1544 | tf_op jit(solution)/shard_map/ppermute | solution.py:29
  185.5 1.3 copy-start.7
  293.9 5.7 %copy-start.2 = (bf16[2048,256]{1,0:T(8,128)(2,1)S(1)}, bf16[2048,256]{1,0:T(8,128)(2,1)}, u32[]{:S(2)}) copy-start(bf16[2048,256]{1,0:T(8,128)(2,1)} %all-gather.5.cloned.1.call-done) | copy-start | bytes 3145732
Sparse Core Ops, SparseCore 0:
  10.3 145.3 all-gather.2
  158.6 135.2 all-gather.4
  310.9 42.6 reduce-scatter.1
